TPU v7x, 32 devices: a whole 2x2x4 slice. The times are simulated.
32 devices in a mesh: fs: 8 (over z, x), tp: 4 (over y, core).
Axes of the slice: x: 2, y: 2, z: 4, core: 2. Of those that a mesh axis runs over, the one named last changes fastest.
Arguments:
- tokens: bfloat16 [1024, 2048], P('fs', 'tp'), may hold values from -6 to 6
- routes: int32 [1024, 2], P('fs'), may hold values from 0 to 3, all different within a row; in each aligned block of 128 rows (0 to 127, 128 to 255, ...) at most 96 rows name the same one
- route_weight: float32 [1024, 2], P('fs'), may hold values from 0.1 to 1
- norm_gain: float32 [2048], P('fs'), may hold values from 0.1 to 1.9
- expert_gate: float32 [4, 2048, 512], P(None, 'fs', 'tp'), may hold values from -0.125 to 0.125
- expert_up: float32 [4, 2048, 512], P(None, 'fs', 'tp'), may hold values from -0.125 to 0.125
- expert_down: float32 [4, 2048, 512], P(None, 'fs', 'tp'), may hold values from -0.25 to 0.25
- shared_gate: float32 [2048, 512], P('fs', 'tp'), may hold values from -0.125 to 0.125
- shared_up: float32 [2048, 512], P('fs', 'tp'), may hold values from -0.125 to 0.125
- shared_down: float32 [512, 2048], P('tp', 'fs'), may hold values from -0.25 to 0.25
Outputs:
- mixed: bfloat16 [1024, 2048], P('fs', 'tp')
- gate_sampler: bfloat16 [8, 2048, 256], P('fs', None, 'tp')
- up_sampler: bfloat16 [8, 2048, 256], P('fs', None, 'tp')
- down_sampler: bfloat16 [8, 2048, 256], P('fs', 'tp')
- shared_gate_out: bfloat16 [2048, 512], P(None, 'tp')
- shared_up_out: bfloat16 [2048, 512], P(None, 'tp')
- shared_down_out: bfloat16 [512, 2048], P('tp')
Inputs may be any that keep to these rules, and one draw needn't show every extreme that they name: `routes`: each row names 2 different experts. In each aligned block of 128 rows no expert is named by more than 96 rows, a bound that some block reaches.
All inputs are finite; a program needn't handle non-finite values.
Results may differ from a plain program's by a relative error of at most 0.009.
Values may be sent and summed in bfloat16 or wider, within the bound.
No kernel may reach another device: no remote copies, remote signals or barrier semaphores. Data moves between devices by JAX's collectives and lax.ppermute only.
A program may use at most 64 MiB of HBM per device.

v0:
```python
import jax
import jax.numpy as jnp
from jax import lax
from jax.sharding import PartitionSpec as P

EPS = 1e-06


def to_owners(matrix, expert_count, unit_count):
    row_share = matrix.shape[1]
    return (
        matrix.reshape(expert_count, row_share, 2, unit_count)
        .transpose(0, 2, 1, 3)
        .reshape(2 * expert_count, row_share, unit_count)
    )


def on_device(
    tokens,
    routes,
    route_weight,
    norm_gain,
    expert_gate,
    expert_up,
    expert_down,
    shared_gate,
    shared_up,
    shared_down,
):
    fs_count = lax.axis_size("fs")
    tp_count = lax.axis_size("tp")
    expert_count, row_share, col_share = expert_gate.shape
    unit_count = col_share // 2
    model_width = row_share * fs_count
    quarter = model_width // tp_count
    tok_count, pick_count = routes.shape
    capacity = 2 * ((3 * tok_count * pick_count + 4 * expert_count - 1) // (4 * expert_count))
    slot_count = fs_count * capacity
    row_gain = norm_gain[None, :, None]
    gate_owned = to_owners((expert_gate * row_gain).astype(jnp.bfloat16), expert_count, unit_count)
    up_owned = to_owners((expert_up * row_gain).astype(jnp.bfloat16), expert_count, unit_count)
    gate_new, up_new = (
        lax.all_to_all(gate_owned, "fs", split_axis=0, concat_axis=1, tiled=True),
        lax.all_to_all(up_owned, "fs", split_axis=0, concat_axis=1, tiled=True),
    )
    down_owned = to_owners(expert_down.astype(jnp.bfloat16), expert_count, unit_count)
    down_new = lax.all_to_all(
        lax.all_to_all(down_owned, "fs", split_axis=0, concat_axis=1, tiled=True),
        "tp",
        split_axis=1,
        concat_axis=2,
        tiled=True,
    )
    shared_gate_new, shared_up_new, shared_down_new = (
        lax.all_gather(
            (shared_gate * norm_gain[:, None]).astype(jnp.bfloat16), "fs", axis=0, tiled=True
        ),
        lax.all_gather(
            (shared_up * norm_gain[:, None]).astype(jnp.bfloat16), "fs", axis=0, tiled=True
        ),
        lax.all_gather(shared_down.astype(jnp.bfloat16), "fs", axis=1, tiled=True),
    )
    gathered = lax.all_gather(tokens, "tp", axis=1, tiled=True)
    tokens_wide = gathered.astype(jnp.float32)
    normed = (
        tokens_wide * lax.rsqrt(jnp.mean(tokens_wide * tokens_wide, axis=1, keepdims=True) + EPS)
    ).astype(jnp.bfloat16)
    shared_act = jnp.dot(normed, shared_gate_new, preferred_element_type=jnp.float32)
    shared_lin = jnp.dot(normed, shared_up_new, preferred_element_type=jnp.float32)
    shared_hidden = (jax.nn.silu(shared_act) * shared_lin).astype(jnp.bfloat16)
    shared_term = jnp.dot(shared_hidden, shared_down_new, preferred_element_type=jnp.float32)
    shared_sum = lax.psum_scatter(
        shared_term.astype(jnp.bfloat16), "tp", scatter_dimension=1, tiled=True
    ).astype(jnp.float32)
    assigned = routes.reshape(-1)
    onehot = (assigned[:, None] == jnp.arange(expert_count, dtype=jnp.int32)[None, :]).astype(
        jnp.int32
    )
    earlier = jnp.cumsum(onehot, axis=0) - onehot
    position = jnp.sum(earlier * onehot, axis=1)
    slot_index = assigned * capacity + position
    token_index = jnp.arange(tok_count * pick_count, dtype=jnp.int32) // pick_count
    slot_token = (
        jnp.full((expert_count * capacity,), tok_count, jnp.int32).at[slot_index].set(token_index)
    )
    padded = jnp.concatenate([normed, jnp.zeros((1, model_width), jnp.bfloat16)], axis=0)
    own_part = lax.dynamic_slice_in_dim(padded, lax.axis_index("tp") * quarter, quarter, 1)
    outgoing = jnp.repeat(
        own_part[slot_token].reshape(expert_count, capacity, quarter), 2, axis=0
    ).reshape(slot_count, quarter)
    arrived = lax.all_to_all(outgoing, "fs", split_axis=0, concat_axis=0, tiled=True)
    portion = lax.all_gather(arrived, "tp", axis=1, tiled=True)
    gate_rows = gate_new[0]
    up_rows = up_new[0]
    gate_act = jnp.dot(portion, gate_rows, preferred_element_type=jnp.float32)
    up_act = jnp.dot(portion, up_rows, preferred_element_type=jnp.float32)
    hidden = (jax.nn.silu(gate_act) * up_act).astype(jnp.bfloat16)
    down_cols = down_new[0]
    half_sum = lax.dot_general(
        lax.all_gather(hidden, "tp", axis=1, tiled=True),
        down_cols,
        (((1,), (1,)), ((), ())),
        preferred_element_type=jnp.float32,
    )
    returned = lax.all_to_all(
        half_sum.astype(jnp.bfloat16), "fs", split_axis=0, concat_axis=0, tiled=True
    )
    pair_sum = jnp.sum(
        returned.astype(jnp.float32).reshape(expert_count, 2, capacity, quarter), axis=1
    ).reshape(expert_count * capacity, quarter)
    gathered_slots = pair_sum[slot_index].reshape(tok_count, pick_count, quarter)
    routed = jnp.sum(gathered_slots * route_weight[:, :, None], axis=1)
    mixed = (shared_sum + routed).astype(jnp.bfloat16)
    return (mixed, gate_new, up_new, down_new, shared_gate_new, shared_up_new, shared_down_new)


def solution(mesh):
    in_specs = (
        P("fs", "tp"),
        P("fs", None),
        P("fs", None),
        P("fs"),
        P(None, "fs", "tp"),
        P(None, "fs", "tp"),
        P(None, "fs", "tp"),
        P("fs", "tp"),
        P("fs", "tp"),
        P("tp", "fs"),
    )
    out_specs = (
        P("fs", "tp"),
        P("fs", None, "tp"),
        P("fs", None, "tp"),
        P("fs", "tp", None),
        P(None, "tp"),
        P(None, "tp"),
        P("tp", None),
    )
    return jax.shard_map(
        on_device, mesh=mesh, in_specs=in_specs, out_specs=out_specs, check_vma=False
    )
```

profile of v0, /device:TPU:0, one launch (start us, length us, event | category | flops | bytes accessed | tf_op | source)
XLA Modules:
  0.0 257.9 jit_solution(7877371888522557811)
XLA Ops:
  7.2 0.8 copy.45
  8.0 0.1 eq.29
  8.1 0.1 eq.25
  8.3 0.7 broadcast_multiply_fusion
  9.0 8.9 %all_gather.18 = bf16[128,2048]{1,0:T(8,128)(2,1)S(1)} all-gather(bf16[128,512]{1,0:T(8,128)(2,1)} %param.10), channel_id=1, replica_groups=mesh['fs'=8,'tp'=4] {'tp'}, dimensions={1}, use_global_device_ids=true | all-gather | bytes 655360 | tf_op jit(solution)/shard_map/all_gather | solution.py:63
  17.8 0.2 fusion.2
  18.0 0.2 fusion.3
  18.2 1.2 reduce-window.6
  19.5 0.1 copy.47
  19.8 0.1 copy.44
  20.0 0.1 mul.94
  20.1 1.4 scatter_custom_fusion
  21.6 2.1 gather_fusion
  23.8 26.3 %all_to_all.75 = bf16[8,96,512]{2,1,0:T(8,128)(2,1)} all-to-all(bf16[8,96,512]{2,1,0:T(8,128)(2,1)S(1)} %bitcast.62), channel_id=1, replica_groups=mesh['fs'=8,'tp'=4] {'fs'}, dimensions={0} | all-to-all | bytes 1572864 | tf_op jit(solution)/shard_map/all_to_all | solution.py:91
  50.2 0.2 multiply_convert_fusion.1
  50.3 0.2 fusion.17
  50.6 0.1 pad_maximum_fusion
  50.7 0.9 copy.50
  51.6 3.6 %all-to-all-start.1 = ((bf16[8,256,64]{1,2,0:T(8,128)(2,1)}), bf16[8,256,64]{1,2,0:T(8,128)(2,1)S(1)}, u32[]{:S(2)}, u32[]{:S(2)}) async-start(bf16[8,256,64]{1,2,0:T(8,128)(2,1)} %copy.50), calls=%async_computation.2 | async-start | bytes 524288 | tf_op jit(solution)/shard_map/all_to_all | solution.py:43
  55.3 0.1 fusion.16
  55.4 0.1 pad_maximum_fusion.2
  55.5 0.9 copy.56
  56.4 7.8 %all-to-all-done.1 = bf16[8,256,64]{1,2,0:T(8,128)(2,1)S(1)} async-done(((bf16[8,256,64]{1,2,0:T(8,128)(2,1)}), bf16[8,256,64]{1,2,0:T(8,128)(2,1)S(1)}, u32[]{:S(2)}, u32[]{:S(2)}) %all-to-all-start.1) | async-done | bytes 262176 | tf_op jit(solution)/shard_map/all_to_all | solution.py:43
  64.2 3.6 %all-to-all-start.3 = ((bf16[8,256,64]{1,2,0:T(8,128)(2,1)}), bf16[8,256,64]{1,2,0:T(8,128)(2,1)S(1)}, u32[]{:S(2)}, u32[]{:S(2)}) async-start(bf16[8,256,64]{1,2,0:T(8,128)(2,1)} %copy.56), calls=%async_computation.4 | async-start | bytes 524288 | tf_op jit(solution)/shard_map/all_to_all | solution.py:48
  67.8 0.1 pad_maximum_fusion.1
  67.9 0.9 copy.53
  68.8 7.6 %all-to-all-done.3 = bf16[8,256,64]{1,2,0:T(8,128)(2,1)S(1)} async-done(((bf16[8,256,64]{1,2,0:T(8,128)(2,1)}), bf16[8,256,64]{1,2,0:T(8,128)(2,1)S(1)}, u32[]{:S(2)}, u32[]{:S(2)}) %all-to-all-start.3) | async-done | bytes 262176 | tf_op jit(solution)/shard_map/all_to_all | solution.py:48
  76.4 3.6 %all-to-all-start.2 = ((bf16[8,256,64]{1,2,0:T(8,128)(2,1)}), bf16[8,256,64]{1,2,0:T(8,128)(2,1)S(1)}, u32[]{:S(2)}, u32[]{:S(2)}) async-start(bf16[8,256,64]{1,2,0:T(8,128)(2,1)} %copy.53), calls=%async_computation.3 | async-start | bytes 524288 | tf_op jit(solution)/shard_map/all_to_all | solution.py:44
  80.1 33.5 %all_gather.19 = bf16[2048,128]{1,0:T(8,128)(2,1)S(1)} all-gather(bf16[256,128]{1,0:T(8,128)(2,1)S(1)} %get-tuple-element.34), channel_id=1, replica_groups=mesh['fs'=8,'tp'=4] {'fs'}, dimensions={0}, use_global_device_ids=true | all-gather | bytes 589824 | tf_op jit(solution)/shard_map/all_gather | solution.py:55
  113.6 0.3 copy.72
  113.9 0.3 reshape.148
  114.2 0.5 broadcast.90
  114.7 11.5 %reduce = bf16[2048,64]{1,0:T(8,128)(2,1)S(1)} reduce(bf16[2048,1,64]{2,1,0:T(2,128)(2,1)S(1)} %bitcast.60, bf16[]{:T(256)} %broadcast.90), dimensions={1}, to_apply=%bitcast.45.reduce_sub_computation | reduce | bytes 524290
  126.2 1.1 reshape.151
  127.3 3.4 %all-to-all-start.4 = ((bf16[4,2,16384]{2,1,0:T(2,128)(2,1)}), bf16[4,2,16384]{2,1,0:T(2,128)(2,1)S(1)}, u32[]{:S(2)}, u32[]{:S(2)}) async-start(bf16[4,2,16384]{2,1,0:T(2,128)(2,1)} %reshape.151), calls=%async_computation.5 | async-start | bytes 524288 | tf_op jit(solution)/shard_map/all_to_all | solution.py:47
  130.8 31.5 %all_gather.20 = bf16[2048,128]{1,0:T(8,128)(2,1)S(1)} all-gather(bf16[256,128]{1,0:T(8,128)(2,1)S(1)} %get-tuple-element.35), channel_id=1, replica_groups=mesh['fs'=8,'tp'=4] {'fs'}, dimensions={0}, use_global_device_ids=true | all-gather | bytes 589824 | tf_op jit(solution)/shard_map/all_gather | solution.py:58
  162.3 0.7 copy.74
  163.0 0.7 copy.75
  163.7 0.6 reshape.152
  164.4 0.6 copy.59
  165.0 0.2 all_to_all.62
  165.3 3.1 %fusion.20 = f32[768,64]{0,1:T(8,128)S(1)} fusion(bf16[768,2048]{1,0:T(8,128)(2,1)} %all-gather.2.cloned.1.call-done, bf16[2048,64]{0,1:T(8,128)(2,1)} %bitcast.71), kind=kOutput, calls=%fused_computation.54 | convolution fusion | flops 201326592 | bytes 3604480 | tf_op jit(solution)/shard_map/dot_general | solution.py:95
  168.4 1.1 fusion
  169.5 7.3 %all_gather.23 = bf16[768,256]{0,1:T(8,128)(2,1)S(1)} all-gather(bf16[768,64]{0,1:T(8,128)(2,1)S(1)} %fusion), channel_id=1, replica_groups=mesh['fs'=8,'tp'=4] {'tp'}, dimensions={1}, use_global_device_ids=true | all-gather | bytes 491520 | tf_op jit(solution)/shard_map/all_gather | solution.py:100
  176.7 1.3 convolution_convert_fusion.1
  178.0 4.3 %all-to-all-start.5 = ((bf16[8,96,512]{2,1,0:T(8,128)(2,1)}), bf16[8,96,512]{2,1,0:T(8,128)(2,1)}, u32[]{:S(2)}, u32[]{:S(2)}) async-start(bf16[8,96,512]{2,1,0:T(8,128)(2,1)} %bitcast.12), calls=%async_computation.6 | async-start | bytes 1572864 | tf_op jit(solution)/shard_map/all_to_all | solution.py:105
  182.4 43.3 %all_gather.21 = bf16[128,2048]{1,0:T(8,128)(2,1)S(1)} all-gather(bf16[128,256]{1,0:T(8,128)(2,1)S(1)} %convert_element_type.61), channel_id=1, replica_groups=mesh['fs'=8,'tp'=4] {'fs'}, dimensions={1}, use_global_device_ids=true | all-gather | bytes 589824 | tf_op jit(solution)/shard_map/all_gather | solution.py:61
  225.7 0.3 fusion.19
  226.0 1.3 convolution_convert_fusion
  227.4 0.1 copy.61
  227.5 0.2 copy.51
  227.7 0.8 all_to_all.66
  228.5 0.1 copy.54
  228.6 0.8 all_to_all.67
  229.5 0.8 copy.65
  230.3 1.4 convert_reduce_fusion
  231.7 1.0 gather_fusion.1
  232.6 0.3 reshape.121
  233.0 0.7 multiply_reduce_fusion
  233.7 13.4 %reduce-scatter.2.cloned.1.call-done = bf16[128,512]{1,0:T(8,128)(2,1)} async-done(((bf16[128,2048]{1,0:T(8,128)(2,1)}), bf16[128,512]{1,0:T(8,128)(2,1)}) %reduce-scatter.2.cloned.1.call-update) | async-done | bytes 131088 | tf_op jit(solution)/shard_map/reduce_scatter | solution.py:72
  247.1 1.6 add_convert_fusion
  248.7 0.8 copy.81
  249.5 0.8 copy.82
  250.3 0.8 copy.83
  (47 shorter events, 0.8 us)
Async XLA Ops:
  7.2 158.1 %all-gather.2.cloned.1.call-start = ((), (), s32[]{:S(2)}) async-start(), calls=%async_computation.8 | async-start | bytes 3932160 | tf_op jit(solution)/shard_map/all_gather | solution.py:92
  21.6 28.5 %copy-start.2 = (f32[4,256,128]{2,1,0:T(8,128)S(1)}, f32[4,256,128]{2,1,0:T(8,128)}, u32[]{:S(2)}) copy-start(f32[4,256,128]{2,1,0:T(8,128)} %param.14) | copy-start | bytes 1572868
  21.6 28.5 %copy-start.3 = (f32[4,256,128]{2,1,0:T(8,128)S(1)}, f32[4,256,128]{2,1,0:T(8,128)}, u32[]{:S(2)}) copy-start(f32[4,256,128]{2,1,0:T(8,128)} %param.15) | copy-start | bytes 1572868
  21.6 28.5 %copy-start.8 = (f32[256]{0:T(256)S(1)}, f32[256]{0:T(256)}, u32[]{:S(2)}) copy-start(f32[256]{0:T(256)} %param.13) | copy-start | bytes 3076
  50.1 5.1 %copy-start.1 = (f32[4,256,128]{2,1,0:T(8,128)S(1)}, f32[4,256,128]{2,1,0:T(8,128)}, u32[]{:S(2)}) copy-start(f32[4,256,128]{2,1,0:T(8,128)} %param.16) | copy-start | bytes 1572868
  51.6 12.6 %all-to-all-start.1 = ((bf16[8,256,64]{1,2,0:T(8,128)(2,1)}), bf16[8,256,64]{1,2,0:T(8,128)(2,1)S(1)}, u32[]{:S(2)}, u32[]{:S(2)}) async-start(bf16[8,256,64]{1,2,0:T(8,128)(2,1)} %copy.50), calls=%async_computation.2 | async-start | bytes 524288 | tf_op jit(solution)/shard_map/all_to_all | solution.py:43
  55.2 13.6 %copy-start.7 = (f32[128,256]{1,0:T(8,128)S(1)}, f32[128,256]{1,0:T(8,128)}, u32[]{:S(2)}) copy-start(f32[128,256]{1,0:T(8,128)} %param.19) | copy-start | bytes 393220
  55.3 24.8 %copy-start.5 = (f32[256,128]{1,0:T(8,128)S(1)}, f32[256,128]{1,0:T(8,128)}, u32[]{:S(2)}) copy-start(f32[256,128]{1,0:T(8,128)} %param.17) | copy-start | bytes 393220
  55.3 24.7 %copy-start.6 = (f32[256,128]{1,0:T(8,128)S(1)}, f32[256,128]{1,0:T(8,128)}, u32[]{:S(2)}) copy-start(f32[256,128]{1,0:T(8,128)} %param.18) | copy-start | bytes 393220
  64.2 12.2 %all-to-all-start.3 = ((bf16[8,256,64]{1,2,0:T(8,128)(2,1)}), bf16[8,256,64]{1,2,0:T(8,128)(2,1)S(1)}, u32[]{:S(2)}, u32[]{:S(2)}) async-start(bf16[8,256,64]{1,2,0:T(8,128)(2,1)} %copy.56), calls=%async_computation.4 | async-start | bytes 524288 | tf_op jit(solution)/shard_map/all_to_all | solution.py:48
  76.4 50.9 %all-to-all-start.2 = ((bf16[8,256,64]{1,2,0:T(8,128)(2,1)}), bf16[8,256,64]{1,2,0:T(8,128)(2,1)S(1)}, u32[]{:S(2)}, u32[]{:S(2)}) async-start(bf16[8,256,64]{1,2,0:T(8,128)(2,1)} %copy.53), calls=%async_computation.3 | async-start | bytes 524288 | tf_op jit(solution)/shard_map/all_to_all | solution.py:44
  127.3 36.4 %all-to-all-start.4 = ((bf16[4,2,16384]{2,1,0:T(2,128)(2,1)}), bf16[4,2,16384]{2,1,0:T(2,128)(2,1)S(1)}, u32[]{:S(2)}, u32[]{:S(2)}) async-start(bf16[4,2,16384]{2,1,0:T(2,128)(2,1)} %reshape.151), calls=%async_computation.5 | async-start | bytes 524288 | tf_op jit(solution)/shard_map/all_to_all | solution.py:47
  165.0 3.4 %copy-start.4 = (bf16[8,8,8,256]{3,2,0,1:T(8,128)(2,1)S(1)}, bf16[8,8,8,256]{3,2,0,1:T(8,128)(2,1)}, u32[]{:S(2)}) copy-start(bf16[8,8,8,256]{3,2,0,1:T(8,128)(2,1)} %copy.75) | copy-start | bytes 786436
  165.2 3.1 %copy-start = (bf16[768,2048]{1,0:T(8,128)(2,1)S(1)}, bf16[768,2048]{1,0:T(8,128)(2,1)}, u32[]{:S(2)}) copy-start(bf16[768,2048]{1,0:T(8,128)(2,1)} %all-gather.2.cloned.1.call-done) | copy-start | bytes 9437188
  178.0 49.4 %copy-start.9 = (f32[128,2]{0,1:T(2,128)S(1)}, f32[128,2]{0,1:T(2,128)}, u32[]{:S(2)}) copy-start(f32[128,2]{0,1:T(2,128)} %param.12) | copy-start | bytes 3076
  178.0 52.3 %all-to-all-start.5 = ((bf16[8,96,512]{2,1,0:T(8,128)(2,1)}), bf16[8,96,512]{2,1,0:T(8,128)(2,1)}, u32[]{:S(2)}, u32[]{:S(2)}) async-start(bf16[8,96,512]{2,1,0:T(8,128)(2,1)} %bitcast.12), calls=%async_computation.6 | async-start | bytes 1572864 | tf_op jit(solution)/shard_map/all_to_all | solution.py:105
  182.4 64.7 %reduce-scatter.2.cloned.1.call-start = ((), (), s32[]{:S(2)}) async-start(), calls=%async_computation.7 | async-start | bytes 655360 | tf_op jit(solution)/shard_map/reduce_scatter | solution.py:72
Sparse Core Ops, SparseCore 0:
  50.2 27.1 all-gather.1
  227.5 19.5 reduce-scatter.1
where the time goes:
time: 259 us; the launch traced here: 258 us
  blocking collectives  151 us (58%)
  waiting for transfers between devices  28.8 us (11%)
  local copies, waits for them, and re-layouts  19.9 us (8%)
  starting transfers between devices  18.7 us (7%)
  other arithmetic  18.2 us (7%)
  between operations  14.4 us (6%)
  matrix products  7.12 us (3%)
    all_gather x1, blocking collectives, on_device(): lax.all_gather(shared_down.astype(jnp.bfloat16), 'fs', axis=1, tiled=True)  43.3 us
    all_gather x1, blocking collectives, on_device(): lax.all_gather((shared_gate * norm_gain[:, None]).astype(jnp.bfloat16), '...  33.5 us
    all_gather x1, blocking collectives, on_device(): lax.all_gather((shared_up * norm_gain[:, None]).astype(jnp.bfloat16), 'fs...  31.5 us
    all_to_all x1, blocking collectives, on_device(): lax.all_to_all(outgoing, 'fs', split_axis=0, concat_axis=0, tiled=True)  26.3 us
    reduce_scatter x1, waiting for transfers between devices, on_device(): lax.psum_scatter(shared_term.astype(jnp.bfloat16), 'tp', scatter_dimensio...  13.4 us
    unnamed x2, other arithmetic  11.6 us
    all_gather x1, blocking collectives, on_device(): gathered = lax.all_gather(tokens, 'tp', axis=1, tiled=True)  8.87 us
    all_to_all x1, waiting for transfers between devices, on_device(): lax.all_to_all(gate_owned, 'fs', split_axis=0, concat_axis=1, tiled=True)  7.75 us
  transfers between devices with their start and end apart: 7, of which 3 were waited for; matrix products, arithmetic and copies ran while one was open for 10% of the time, Pallas kernels for 0%

commit v1 on v0

--- a/solution.py
+++ b/solution.py
@@ -44,13 +44,20 @@
         lax.all_to_all(up_owned, "fs", split_axis=0, concat_axis=1, tiled=True),
     )
     down_owned = to_owners(expert_down.astype(jnp.bfloat16), expert_count, unit_count)
-    down_new = lax.all_to_all(
-        lax.all_to_all(down_owned, "fs", split_axis=0, concat_axis=1, tiled=True),
-        "tp",
-        split_axis=1,
-        concat_axis=2,
-        tiled=True,
-    )
+    x = lax.all_to_all(down_owned, "fs", split_axis=0, concat_axis=1, tiled=True)
+    ways, here = (lax.axis_size("tp"), lax.axis_index("tp"))
+    width = x.shape[1] // ways
+    lengths = list(x.shape)
+    lengths[1] = width
+    height = lengths[2]
+    lengths[2] = height * ways
+    full = jnp.zeros(lengths, x.dtype)
+    for mask in range(ways):
+        part = lax.dynamic_slice_in_dim(x, (here ^ mask) * width, width, axis=1)
+        if mask:
+            part = lax.ppermute(part, "tp", [(d, d ^ mask) for d in range(ways)])
+        full = lax.dynamic_update_slice_in_dim(full, part, (here ^ mask) * height, axis=2)
+    down_new = full
     shared_gate_new, shared_up_new, shared_down_new = (
         lax.all_gather(
             (shared_gate * norm_gain[:, None]).astype(jnp.bfloat16), "fs", axis=0, tiled=True

time: 259 us -> 243 us (0.938)
  other arithmetic: 18.2 us -> 6.68 us
    unnamed x2 -> x1, other arithmetic: 11.6 us -> 0.07 us
    all_gather x1, blocking collectives: 33.5 us -> 43.3 us  [on_device(): lax.all_gather((shared_gate * norm_gain[:, None]).astype(jnp.bfloat16), '...]
    all_gather x1, blocking collectives: 43.3 us -> 33.7 us  [on_device(): lax.all_gather(shared_down.astype(jnp.bfloat16), 'fs', axis=1, tiled=True)]
    all_to_all x1, waiting for transfers between devices: 0.01 us -> 7.75 us  [on_device(): lax.all_to_all(up_owned, 'fs', split_axis=0, concat_axis=1, tiled=True)]
    all_to_all x1, waiting for transfers between devices: 7.75 us -> 0.01 us  [on_device(): lax.all_to_all(gate_owned, 'fs', split_axis=0, concat_axis=1, tiled=True)]
    all_to_all x1 -> x0, starting transfers between devices: 3.41 us -> none  [on_device(): lax.all_to_all(lax.all_to_all(down_owned, 'fs', split_axis=0, concat_axis...]
    unnamed x29 -> x25, local copies, waits for them, and re-layouts: 6.41 us -> 3.33 us
    dynamic_update_slice x0 -> x4, local copies, waits for them, and re-layouts: none -> 2.64 us  [on_device(): lax.dynamic_update_slice_in_dim(full, part, (here ^ mask) * height, axis=2)]
  transfers between devices with their start and end apart: 7 -> 9, of which waited for: 3 -> 3; matrix products, arithmetic and copies ran while one was open for 10% -> 5% of each run, Pallas kernels for 0% -> 0%
where the time goes in v1:
time: 243 us
  blocking collectives  150 us (62%)
  waiting for transfers between devices  29.5 us (12%)
  local copies, waits for them, and re-layouts  18.1 us (7%)
  starting transfers between devices  17.1 us (7%)
  between operations  14.5 us (6%)
  matrix products  7.13 us (3%)
  other arithmetic  6.68 us (3%)
    all_gather x1, blocking collectives, on_device(): lax.all_gather((shared_gate * norm_gain[:, None]).astype(jnp.bfloat16), '...  43.3 us
    all_gather x1, blocking collectives, on_device(): lax.all_gather(shared_down.astype(jnp.bfloat16), 'fs', axis=1, tiled=True)  33.7 us
    all_gather x1, blocking collectives, on_device(): lax.all_gather((shared_up * norm_gain[:, None]).astype(jnp.bfloat16), 'fs...  31.5 us
    all_to_all x1, blocking collectives, on_device(): lax.all_to_all(outgoing, 'fs', split_axis=0, concat_axis=0, tiled=True)  26.3 us
    reduce_scatter x1, waiting for transfers between devices, on_device(): lax.psum_scatter(shared_term.astype(jnp.bfloat16), 'tp', scatter_dimensio...  14.2 us
    all_gather x1, blocking collectives, on_device(): gathered = lax.all_gather(tokens, 'tp', axis=1, tiled=True)  8.89 us
    all_to_all x1, waiting for transfers between devices, on_device(): lax.all_to_all(up_owned, 'fs', split_axis=0, concat_axis=1, tiled=True)  7.75 us
    all_to_all x1, waiting for transfers between devices, on_device(): lax.all_to_all(down_owned, 'fs', split_axis=0, concat_axis=1, tiled=True)  7.45 us
  transfers between devices with their start and end apart: 9, of which 3 were waited for; matrix products, arithmetic and copies ran while one was open for 5% of the time, Pallas kernels for 0%

profile of v1, /device:TPU:0, one launch (start us, length us, event | category | flops | bytes accessed | tf_op | source)
XLA Modules:
  0.0 242.7 jit_solution(5952156706258513152)
XLA Ops:
  7.2 0.7 broadcast_multiply_fusion
  7.9 0.8 copy.37
  8.7 0.1 eq.29
  8.8 0.1 eq.25
  9.0 8.9 %all_gather.18 = bf16[128,2048]{1,0:T(8,128)(2,1)S(1)} all-gather(bf16[128,512]{1,0:T(8,128)(2,1)} %param.10), channel_id=1, replica_groups=mesh['fs'=8,'tp'=4] {'tp'}, dimensions={1}, use_global_device_ids=true | all-gather | bytes 655360 | tf_op jit(solution)/shard_map/all_gather | solution.py:70
  17.9 0.2 fusion.2
  18.1 0.2 fusion.3
  18.2 0.1 copy.36
  18.3 0.1 mul.116
  18.5 1.2 reduce-window.6
  20.1 1.4 scatter_custom_fusion
  21.6 2.1 gather_fusion
  23.8 26.3 %all_to_all.57 = bf16[8,96,512]{2,1,0:T(8,128)(2,1)} all-to-all(bf16[8,96,512]{2,1,0:T(8,128)(2,1)S(1)} %bitcast.57), channel_id=1, replica_groups=mesh['fs'=8,'tp'=4] {'fs'}, dimensions={0} | all-to-all | bytes 1572864 | tf_op jit(solution)/shard_map/all_to_all | solution.py:98
  50.2 0.2 multiply_convert_fusion.1
  50.3 0.2 fusion.18
  50.6 0.1 pad_maximum_fusion.1
  50.7 0.9 copy.45
  51.6 3.6 %all-to-all-start.2 = ((bf16[8,256,64]{1,2,0:T(8,128)(2,1)}), bf16[8,256,64]{1,2,0:T(8,128)(2,1)S(1)}, u32[]{:S(2)}, u32[]{:S(2)}) async-start(bf16[8,256,64]{1,2,0:T(8,128)(2,1)} %copy.45), calls=%async_computation.3 | async-start | bytes 524288 | tf_op jit(solution)/shard_map/all_to_all | solution.py:44
  55.3 0.1 fusion.17
  55.5 0.1 pad_maximum_fusion.2
  55.6 0.9 copy.48
  56.5 7.8 %all-to-all-done.2 = bf16[8,256,64]{1,2,0:T(8,128)(2,1)S(1)} async-done(((bf16[8,256,64]{1,2,0:T(8,128)(2,1)}), bf16[8,256,64]{1,2,0:T(8,128)(2,1)S(1)}, u32[]{:S(2)}, u32[]{:S(2)}) %all-to-all-start.2) | async-done | bytes 262176 | tf_op jit(solution)/shard_map/all_to_all | solution.py:44
  64.2 3.6 %all-to-all-start.3 = ((bf16[8,256,64]{1,2,0:T(8,128)(2,1)}), bf16[8,256,64]{1,2,0:T(8,128)(2,1)S(1)}, u32[]{:S(2)}, u32[]{:S(2)}) async-start(bf16[8,256,64]{1,2,0:T(8,128)(2,1)} %copy.48), calls=%async_computation.4 | async-start | bytes 524288 | tf_op jit(solution)/shard_map/all_to_all | solution.py:47
  67.8 0.1 pad_maximum_fusion
  67.9 0.9 copy.42
  69.0 7.5 %all-to-all-done.3 = bf16[8,256,64]{1,2,0:T(8,128)(2,1)S(1)} async-done(((bf16[8,256,64]{1,2,0:T(8,128)(2,1)}), bf16[8,256,64]{1,2,0:T(8,128)(2,1)S(1)}, u32[]{:S(2)}, u32[]{:S(2)}) %all-to-all-start.3) | async-done | bytes 262176 | tf_op jit(solution)/shard_map/all_to_all | solution.py:47
  76.4 3.6 %all-to-all-start.1 = ((bf16[8,256,64]{1,2,0:T(8,128)(2,1)}), bf16[8,256,64]{1,2,0:T(8,128)(2,1)S(1)}, u32[]{:S(2)}, u32[]{:S(2)}) async-start(bf16[8,256,64]{1,2,0:T(8,128)(2,1)} %copy.42), calls=%async_computation.2 | async-start | bytes 524288 | tf_op jit(solution)/shard_map/all_to_all | solution.py:43
  80.0 33.7 %all_gather.21 = bf16[128,2048]{1,0:T(8,128)(2,1)S(1)} all-gather(bf16[128,256]{1,0:T(8,128)(2,1)S(1)} %convert_element_type.61), channel_id=1, replica_groups=mesh['fs'=8,'tp'=4] {'fs'}, dimensions={1}, use_global_device_ids=true | all-gather | bytes 589824 | tf_op jit(solution)/shard_map/all_gather | solution.py:68
  113.7 0.1 copy.49
  113.9 0.1 all_to_all.47
  114.0 0.7 constant_dynamic-slice_fusion
  114.6 1.1 collective-permute-start.1
  115.7 0.8 collective-permute-start.2
  116.5 31.5 %all_gather.20 = bf16[2048,128]{1,0:T(8,128)(2,1)S(1)} all-gather(bf16[256,128]{1,0:T(8,128)(2,1)S(1)} %get-tuple-element.18), channel_id=1, replica_groups=mesh['fs'=8,'tp'=4] {'fs'}, dimensions={0}, use_global_device_ids=true | all-gather | bytes 589824 | tf_op jit(solution)/shard_map/all_gather | solution.py:65
  148.0 0.1 copy.50
  148.2 0.5 dynamic_update_slice.12
  148.7 0.1 copy.51
  148.8 0.9 dynamic_update_slice.13
  149.7 0.1 copy.52
  149.9 0.4 dynamic_update_slice.14
  150.3 0.1 copy.53
  150.4 0.8 dynamic_update_slice.15
  151.3 3.1 %fusion.21 = f32[768,64]{0,1:T(8,128)S(1)} fusion(bf16[768,2048]{1,0:T(8,128)(2,1)} %all-gather.2.cloned.1.call-done, bf16[2048,64]{0,1:T(8,128)(2,1)S(1)} %bitcast.64), kind=kOutput, calls=%fused_computation.59 | convolution fusion | flops 201326592 | bytes 3604480 | tf_op jit(solution)/shard_map/dot_general | solution.py:102
  154.4 1.1 fusion
  155.5 6.1 %all_gather.23 = bf16[768,256]{0,1:T(8,128)(2,1)S(1)} all-gather(bf16[768,64]{0,1:T(8,128)(2,1)S(1)} %fusion), channel_id=1, replica_groups=mesh['fs'=8,'tp'=4] {'tp'}, dimensions={1}, use_global_device_ids=true | all-gather | bytes 491520 | tf_op jit(solution)/shard_map/all_gather | solution.py:107
  161.6 1.3 convolution_convert_fusion.1
  163.0 4.3 %all-to-all-start.4 = ((bf16[8,96,512]{2,1,0:T(8,128)(2,1)}), bf16[8,96,512]{2,1,0:T(8,128)(2,1)}, u32[]{:S(2)}, u32[]{:S(2)}) async-start(bf16[8,96,512]{2,1,0:T(8,128)(2,1)} %bitcast.11), calls=%async_computation.5 | async-start | bytes 1572864 | tf_op jit(solution)/shard_map/all_to_all | solution.py:112
  167.4 43.3 %all_gather.19 = bf16[2048,128]{1,0:T(8,128)(2,1)S(1)} all-gather(bf16[256,128]{1,0:T(8,128)(2,1)S(1)} %get-tuple-element.17), channel_id=1, replica_groups=mesh['fs'=8,'tp'=4] {'fs'}, dimensions={0}, use_global_device_ids=true | all-gather | bytes 589824 | tf_op jit(solution)/shard_map/all_gather | solution.py:62
  210.7 0.3 fusion.20
  211.0 1.3 convolution_convert_fusion
  212.3 0.1 copy.54
  212.5 0.2 copy.43
  212.6 0.8 all_to_all.50
  213.4 0.1 copy.46
  213.6 0.8 all_to_all.51
  214.4 1.4 convert_reduce_fusion
  215.8 1.0 gather_fusion.1
  216.7 0.3 reshape.120
  217.1 0.7 multiply_reduce_fusion
  217.8 14.2 %reduce-scatter.2.cloned.1.call-done = bf16[128,512]{1,0:T(8,128)(2,1)} async-done(((bf16[128,2048]{1,0:T(8,128)(2,1)}), bf16[128,512]{1,0:T(8,128)(2,1)}) %reduce-scatter.2.cloned.1.call-update) | async-done | bytes 131088 | tf_op jit(solution)/shard_map/reduce_scatter | solution.py:79
  231.9 1.6 add_convert_fusion
  233.5 0.8 copy.74
  234.3 0.8 copy.75
  235.1 0.8 copy.76
  (53 shorter events, 0.9 us)
Async XLA Ops:
  7.2 144.1 %all-gather.2.cloned.1.call-start = ((), (), s32[]{:S(2)}) async-start(), calls=%async_computation.7 | async-start | bytes 3932160 | tf_op jit(solution)/shard_map/all_gather | solution.py:99
  21.6 28.5 %copy-start.3 = (f32[4,256,128]{2,1,0:T(8,128)S(1)}, f32[4,256,128]{2,1,0:T(8,128)}, u32[]{:S(2)}) copy-start(f32[4,256,128]{2,1,0:T(8,128)} %param.14) | copy-start | bytes 1572868
  21.6 28.5 %copy-start.4 = (f32[4,256,128]{2,1,0:T(8,128)S(1)}, f32[4,256,128]{2,1,0:T(8,128)}, u32[]{:S(2)}) copy-start(f32[4,256,128]{2,1,0:T(8,128)} %param.15) | copy-start | bytes 1572868
  21.6 28.5 %copy-start.8 = (f32[256]{0:T(256)S(1)}, f32[256]{0:T(256)}, u32[]{:S(2)}) copy-start(f32[256]{0:T(256)} %param.13) | copy-start | bytes 3076
  50.2 5.1 %copy-start.2 = (f32[4,256,128]{2,1,0:T(8,128)S(1)}, f32[4,256,128]{2,1,0:T(8,128)}, u32[]{:S(2)}) copy-start(f32[4,256,128]{2,1,0:T(8,128)} %param.16) | copy-start | bytes 1572868
  51.6 12.6 %all-to-all-start.2 = ((bf16[8,256,64]{1,2,0:T(8,128)(2,1)}), bf16[8,256,64]{1,2,0:T(8,128)(2,1)S(1)}, u32[]{:S(2)}, u32[]{:S(2)}) async-start(bf16[8,256,64]{1,2,0:T(8,128)(2,1)} %copy.45), calls=%async_computation.3 | async-start | bytes 524288 | tf_op jit(solution)/shard_map/all_to_all | solution.py:44
  55.2 13.6 %copy-start.7 = (f32[128,256]{1,0:T(8,128)S(1)}, f32[128,256]{1,0:T(8,128)}, u32[]{:S(2)}) copy-start(f32[128,256]{1,0:T(8,128)} %param.19) | copy-start | bytes 393220
  55.2 13.6 %copy-start.5 = (f32[256,128]{1,0:T(8,128)S(1)}, f32[256,128]{1,0:T(8,128)}, u32[]{:S(2)}) copy-start(f32[256,128]{1,0:T(8,128)} %param.17) | copy-start | bytes 393220
  55.3 13.6 %copy-start.6 = (f32[256,128]{1,0:T(8,128)S(1)}, f32[256,128]{1,0:T(8,128)}, u32[]{:S(2)}) copy-start(f32[256,128]{1,0:T(8,128)} %param.18) | copy-start | bytes 393220
  64.2 12.2 %all-to-all-start.3 = ((bf16[8,256,64]{1,2,0:T(8,128)(2,1)}), bf16[8,256,64]{1,2,0:T(8,128)(2,1)S(1)}, u32[]{:S(2)}, u32[]{:S(2)}) async-start(bf16[8,256,64]{1,2,0:T(8,128)(2,1)} %copy.48), calls=%async_computation.4 | async-start | bytes 524288 | tf_op jit(solution)/shard_map/all_to_all | solution.py:47
  76.4 71.6 %all-to-all-start.1 = ((bf16[8,256,64]{1,2,0:T(8,128)(2,1)}), bf16[8,256,64]{1,2,0:T(8,128)(2,1)S(1)}, u32[]{:S(2)}, u32[]{:S(2)}) async-start(bf16[8,256,64]{1,2,0:T(8,128)(2,1)} %copy.42), calls=%async_computation.2 | async-start | bytes 524288 | tf_op jit(solution)/shard_map/all_to_all | solution.py:43
  114.6 34.0 %collective-permute-start = (bf16[1,512,64]{1,2,0:T(8,128)(2,1)}, bf16[1,512,64]{1,2,0:T(8,128)(2,1)S(1)}, u32[]{:S(2)}, u32[]{:S(2)}) collective-permute-start(bf16[1,512,64]{1,2,0:T(8,128)(2,1)} %get-tuple-element.9), channel_id=1, source_target_pairs={{0,1},{1,0},{2,3},{3,2},{4,5},{5,4},{6,7},{7,6},{8,9},{9,8},{10,11... | collective-permute-start | bytes 196616 | tf_op jit(solution)/shard_map/ppermute | solution.py:58
  114.6 35.1 %collective-permute-start.1 = (bf16[1,512,64]{1,2,0:T(8,128)(2,1)S(1)}, bf16[1,512,64]{1,2,0:T(8,128)(2,1)S(1)}, u32[]{:S(2)}, u32[]{:S(2)}) collective-permute-start(bf16[1,512,64]{1,2,0:T(8,128)(2,1)S(1)} %get-tuple-element.8), channel_id=1, source_target_pairs={{0,2},{1,3},{2,0},{3,1},{4,6},{5,7},{6,4},{7,5},{8,10},{9,11},{10,... | collective-permute-start | bytes 196616 | tf_op jit(solution)/shard_map/ppermute | solution.py:58
  115.7 34.6 %collective-permute-start.2 = (bf16[1,512,64]{1,2,0:T(8,128)(2,1)S(1)}, bf16[1,512,64]{1,2,0:T(8,128)(2,1)S(1)}, u32[]{:S(2)}, u32[]{:S(2)}) collective-permute-start(bf16[1,512,64]{1,2,0:T(8,128)(2,1)S(1)} %get-tuple-element.7), channel_id=1, source_target_pairs={{0,3},{1,2},{2,1},{3,0},{4,7},{5,6},{6,5},{7,4},{8,11},{9,10},{10,... | collective-permute-start | bytes 196616 | tf_op jit(solution)/shard_map/ppermute | solution.py:58
  151.3 10.4 %copy-start.1 = (bf16[1,512,256]{2,1,0:T(8,128)(2,1)}, bf16[1,512,256]{2,1,0:T(8,128)(2,1)S(1)}, u32[]{:S(2)}) copy-start(bf16[1,512,256]{2,1,0:T(8,128)(2,1)S(1)} %dynamic_update_slice.15) | copy-start | bytes 786436
  151.3 3.1 %copy-start = (bf16[768,2048]{1,0:T(8,128)(2,1)S(1)}, bf16[768,2048]{1,0:T(8,128)(2,1)}, u32[]{:S(2)}) copy-start(bf16[768,2048]{1,0:T(8,128)(2,1)} %all-gather.2.cloned.1.call-done) | copy-start | bytes 9437188
  163.0 49.3 %copy-start.9 = (f32[128,2]{0,1:T(2,128)S(1)}, f32[128,2]{0,1:T(2,128)}, u32[]{:S(2)}) copy-start(f32[128,2]{0,1:T(2,128)} %param.12) | copy-start | bytes 3076
  163.0 51.4 %all-to-all-start.4 = ((bf16[8,96,512]{2,1,0:T(8,128)(2,1)}), bf16[8,96,512]{2,1,0:T(8,128)(2,1)}, u32[]{:S(2)}, u32[]{:S(2)}) async-start(bf16[8,96,512]{2,1,0:T(8,128)(2,1)} %bitcast.11), calls=%async_computation.5 | async-start | bytes 1572864 | tf_op jit(solution)/shard_map/all_to_all | solution.py:112
  167.3 64.6 %reduce-scatter.2.cloned.1.call-start = ((), (), s32[]{:S(2)}) async-start(), calls=%async_computation.6 | async-start | bytes 655360 | tf_op jit(solution)/shard_map/reduce_scatter | solution.py:79
Sparse Core Ops, SparseCore 0:
  50.3 27.1 all-gather.1
  212.4 19.4 reduce-scatter.1
